TPU v7x, 256 devices: a whole 4x4x8 slice. The times are simulated.
256 devices in a mesh: rep: 64 (over z, y, core), fs: 2 (over x_lo), tp: 2 (over x_hi).
Axes of the slice: x: 4 (x_hi: 2, x_lo: 2; x = x_hi * 2 + x_lo), y: 4, z: 8, core: 2. Of those that a mesh axis runs over, the one named last changes fastest.
Arguments:
- inputs: bfloat16 [32768, 2048], P(('rep', 'tp'), 'fs'), may hold values from -6 to 6
- pre_act: bfloat16 [32768, 4096], P(('rep', 'fs'), 'tp'), may hold values from -6 to 6
- cotangent: bfloat16 [32768, 2048], P(('rep', 'tp'), 'fs'), may hold values from -24 to 24
- up_weight: bfloat16 [2048, 4096], P('fs', 'tp'), may hold values from -0.125 to 0.125
- down_weight: bfloat16 [4096, 2048], P('tp', 'fs'), may hold values from -0.09375 to 0.09375
Outputs:
- grad_inputs: bfloat16 [32768, 2048], P(('rep', 'tp'), 'fs')
- grad_up: float32 [2048, 4096], P('fs', 'tp')
- grad_down: float32 [4096, 2048], P('tp', 'fs')
All inputs are finite; a program needn't handle non-finite values.
Results may differ from a plain program's by a relative error of at most 0.015.
Values may be sent and summed in bfloat16 or wider, within the bound.
No kernel may reach another device: no remote copies, remote signals or barrier semaphores. Data moves between devices by JAX's collectives and lax.ppermute only.
A program may use at most 128 MiB of HBM per device.

v0:
```python
import jax
import jax.numpy as jnp
from jax import lax
from jax.experimental import pallas as pl
from jax.experimental.pallas import tpu as pltpu
from jax.sharding import Mesh
from jax.sharding import PartitionSpec as P


NY = 4
NC = 2
AXES = ("z", "y", "c", "fs", "tp")
REP = ("z", "y", "c")


def send(value, y=0, c=0, fs=0, tp=0):
    sizes = [lax.axis_size(axis) for axis in AXES]
    flips = (0, y, c, fs, tp)
    pairs = []
    total = 1
    for size in sizes:
        total *= size
    for source in range(total):
        rest, at = source, []
        for size in reversed(sizes):
            at.append(rest % size)
            rest //= size
        target = 0
        for size, place, flip in zip(sizes, reversed(at), flips):
            target = target * size + (place ^ flip)
        pairs.append((source, target))
    return lax.ppermute(value, AXES, pairs)


def exchange(value, axis):
    return lax.all_to_all(value, axis, 0, 0, tiled=True)


def to_all(value, axis):
    peers = lax.axis_size(axis)
    return exchange(jnp.broadcast_to(value[None], (peers, *value.shape)), axis)


def added(*values):
    total = values[0].astype(jnp.float32)
    for value in values[1:]:
        total = total + value.astype(jnp.float32)
    return total.astype(jnp.bfloat16)


def rows_of(value, start, size):
    return lax.dynamic_slice_in_dim(value, start, size, axis=0)


def cols_of(value, start, size):
    return lax.dynamic_slice_in_dim(value, start, size, axis=1)


def ordered(flag, own, other):
    return jnp.where(flag, other, own), jnp.where(flag, own, other)


def ring_sum(own, near, far, diag):
    return added(own, send(near, fs=1), send(diag, fs=1, tp=1), send(far, tp=1))


def contract_rows(left, right):
    return lax.dot_general(left, right, (((0,), (0,)), ((), ())), preferred_element_type=jnp.float32)


def contract_cols(left, right):
    return lax.dot_general(left, right, (((1,), (1,)), ((), ())), preferred_element_type=jnp.float32)


def tokens_of(own, near, far, diag):
    return jnp.concatenate([jnp.concatenate([own, near], 1), jnp.concatenate([far, diag], 1)], 0)


CHUNKS = ((2, 0), (1, 0), (2, 1), (3, 1), (1, 1), (3, 0), (0, 0), (0, 1))


def chunk_sums(y, own, partner, halves_first):
    rows, columns = own.shape[2:]
    at = jnp.stack([part for flip, half in CHUNKS for part in (y ^ flip, half)]).astype(jnp.int32)

    def kernel(at, own, partner, one, three, rest):
        total = (own[0].astype(jnp.float32) + partner[0].astype(jnp.float32)).astype(jnp.bfloat16)
        step = pl.program_id(0)
        for target, low, high in ((one, 0, 2), (three, 2, 4), (rest, 4, 8)):

            @pl.when((step >= low) & (step < high))
            def _(target=target):
                target[...] = total

    def source(i, at):
        return (at[2 * i + 1], at[2 * i], 0, 0) if halves_first else (at[2 * i], at[2 * i + 1], 0, 0)

    def target(low, high):
        return pl.BlockSpec((1, rows, columns), lambda i, at: (jnp.clip(i - low, 0, high - low - 1), 0, 0))

    return pl.pallas_call(
        kernel,
        grid_spec=pltpu.PrefetchScalarGridSpec(
            num_scalar_prefetch=1,
            grid=(len(CHUNKS),),
            in_specs=[pl.BlockSpec((1, 1, rows, columns), source)] * 2,
            out_specs=[target(0, 2), target(2, 4), target(4, 8)],
        ),
        out_shape=[jax.ShapeDtypeStruct((n, rows, columns), jnp.bfloat16) for n in (2, 2, 4)],
        cost_estimate=pl.CostEstimate(flops=own.size, bytes_accessed=own.size * 6, transcendentals=0),
    )(at, own, partner)


def laid(out, group, c, shape, by_rows, scale):
    places, own, partner = group
    count, nz, nf, rows, columns = partner.shape
    at = jnp.concatenate([places, c[None]]).astype(jnp.int32)

    def kernel(at, *refs):
        target = refs[-1]

        def put(source, core):
            def step(i, _):
                z, f = i // nf, i % nf
                wide = source[z, f].astype(jnp.float32) * scale
                lines = pl.ds(pl.multiple_of(z * rows, rows), rows)
                if by_rows:
                    target[f, core, 0, lines] = wide
                else:
                    left = pl.multiple_of((f * NC + core) * columns, columns)
                    target[lines, pl.ds(left, columns)] = wide
                return _

            lax.fori_loop(0, nz * nf, step, 0)

        for index in range(count):

            @pl.when(pl.program_id(0) == index)
            def _(source=refs[index]):
                put(source, at[count])

        put(refs[count].at[0], 1 - at[count])

    arguments = (at, *own, partner) + (() if out is None else (out,))
    specs = [pl.BlockSpec((nz, nf, rows, columns), lambda i, at: (0, 0, 0, 0)) for _ in own]
    specs += [pl.BlockSpec((1, nz, nf, rows, columns), lambda i, at: (i, 0, 0, 0, 0))]
    specs += [] if out is None else [pl.BlockSpec(memory_space=pl.ANY)]
    if by_rows:
        out_spec = pl.BlockSpec((nf, NC, 1, nz * rows, columns), lambda i, at: (0, 0, at[i], 0, 0))
    else:
        out_spec = pl.BlockSpec((nz * rows, nf * NC * columns), lambda i, at: (at[i], 0))
    return pl.pallas_call(
        kernel,
        grid_spec=pltpu.PrefetchScalarGridSpec(
            num_scalar_prefetch=1, grid=(count,), in_specs=specs, out_specs=out_spec
        ),
        out_shape=jax.ShapeDtypeStruct(shape, jnp.float32),
        input_output_aliases={} if out is None else {count + 2: 0},
        cost_estimate=pl.CostEstimate(
            flops=2 * partner.size, bytes_accessed=partner.size * 12, transcendentals=0
        ),
    )(*arguments)


def per_device(inputs, pre_act, cotangent, up_weight, down_weight):
    nz = lax.axis_size("z")
    z, y, c, fs, tp = (lax.axis_index(axis) for axis in AXES)
    width = pre_act.shape[1]
    quarter, eighth = width // 2, width // 4
    half_d = inputs.shape[1]
    rows = inputs.shape[0]
    factor = (rows * nz * NY * NC * 2) ** (-0.5)
    mine, theirs = fs * quarter, (1 - fs) * quarter
    first, second = c * eighth, (1 - c) * eighth
    rows_down, rows_up = eighth // (NY * nz), half_d // (NY * nz)
    fixed = lax.optimization_barrier

    def cols_by_core(value, start):
        return jnp.concatenate([cols_of(value, start + first, eighth), cols_of(value, start + second, eighth)], 1)

    down_near = rows_of(down_weight, theirs + first + y * (eighth // NY), eighth // NY)
    cot_near = send(jnp.concatenate([cotangent, down_near]), fs=1)
    cot_near, down_near = fixed((cot_near[:rows], cot_near[rows:]))
    cot_diag = send(cotangent, fs=1, tp=1)
    pre_near = send(cols_by_core(pre_act, theirs), fs=1)
    down_near = to_all(down_near, "y").reshape(eighth, half_d)
    down_other = send(down_near, c=1)
    cot_far = send(cot_near, fs=1, tp=1)
    in_near = send(inputs, fs=1)
    in_diag = send(inputs, fs=1, tp=1)
    in_far = send(inputs, tp=1)
    up_near = send(cols_of(up_weight, theirs + first, eighth), fs=1)
    up_other = send(up_near, c=1)

    down_own = fixed(
        jnp.concatenate(
            [rows_of(down_weight, mine + first, eighth), rows_of(down_weight, mine + second, eighth)]
        )
    )
    cot = fixed(tokens_of(cotangent, cot_near, cot_far, cot_diag))
    pre = jnp.concatenate(ordered(fs != tp, cols_by_core(pre_act, mine), pre_near), 0)
    positive = jnp.maximum(pre.astype(jnp.float32), 0.0)
    square = fixed(
        tuple((p * p).astype(jnp.bfloat16) for p in (positive[:, :eighth], positive[:, eighth:]))
    )
    down_part = contract_rows(square[0], cot).astype(jnp.bfloat16)
    down_parts = (down_part, send(contract_rows(square[1], cot).astype(jnp.bfloat16), c=1))

    split = (NY, 2, eighth // NY // 2, 2 * half_d)
    down_sums = chunk_sums(y, *[part.reshape(split) for part in down_parts], False)

    down = fixed(jnp.concatenate([down_own, fixed(jnp.concatenate([down_near, down_other]))], 1))
    grad_pre = fixed((2.0 * positive * contract_cols(cot, down)).astype(jnp.bfloat16))
    grad_pre, *ready = fixed((grad_pre, inputs, in_near, in_far, in_diag, down_sums[0][0, :1]))[:5]
    x = fixed(tokens_of(*ready))
    up_parts = tuple(
        contract_rows(x, g).astype(jnp.bfloat16) for g in (grad_pre[:, :eighth], grad_pre[:, eighth:])
    )
    up_parts = (up_parts[0], send(up_parts[1], c=1))

    split = (2, NY, half_d // NY, eighth)
    up_sums = chunk_sums(y, *[part.reshape(split) for part in up_parts], True)

    def y_sum(one, three, rest):
        one = send(one, y=1)
        three = send(three, y=3)
        right = send(added(rest[0], three[0]), y=1)
        left = send(added(rest[1], one[0]), y=3)
        return added(rest[2], one[1], left), added(rest[3], three[1], right)

    def z_sum(value):
        got = exchange(value, "z")
        return added(*[got[i] for i in range(nz)])

    def gathered(own, other):
        both = jnp.stack(ordered(fs == 1, own, send(other, fs=1)))
        value = to_all(both, "z").reshape(nz, *both.shape)
        ways = ((y ^ 1, 1), (y ^ 3, 3), (y ^ 2, 2))
        found = [(y, value)] + [(at, send(value, y=flip)) for at, flip in ways]
        near, far = [v for _, v in found[:3]], found[3][1]
        passed = send(jnp.stack(near), c=1)
        places = jnp.stack([at for at, _ in found])
        return (places[:3], near, passed), (places[3:], [far], send(far, c=1)[None])

    d = jnp.concatenate(y_sum(*down_sums)).reshape(nz, rows_down, 2 * half_d)
    d = z_sum(d)
    u = jnp.stack([half.reshape(nz, rows_up, eighth) for half in y_sum(*up_sums)], 1)
    u = z_sum(u)
    near, far = gathered(d[:, :half_d], d[:, half_d:])
    shape = (2, NC, NY, nz * rows_down, half_d)
    grad_down = laid(None, near, c, shape, True, factor)
    grad_down = laid(grad_down, far, c, shape, True, factor)
    near, far = gathered(u[0], u[1])
    grad_up = laid(None, near, c, (half_d, width), False, factor)
    grad_up = laid(grad_up, far, c, (half_d, width), False, factor)

    up_own = fixed(cols_by_core(up_weight, mine))
    up = fixed(jnp.concatenate([up_own, fixed(jnp.concatenate([up_near, up_other], 1))]))
    part = lax.map(lambda r: contract_cols(r, up).astype(jnp.bfloat16), grad_pre.reshape(4, rows // 2, quarter))
    part = part.reshape(2 * rows, 2 * half_d)
    grad_inputs = ring_sum(
        part[:rows, :half_d],
        part[:rows, half_d:],
        part[rows:, :half_d],
        part[rows:, half_d:],
    )
    return grad_inputs, grad_up, grad_down.reshape(width, half_d)


def solution(mesh):
    reps = mesh.shape["rep"]
    split = Mesh(mesh.devices.reshape(reps // (NY * NC), NY, NC, 2, 2), AXES)
    tokens = P((*REP, "tp"), "fs")

    return jax.shard_map(
        per_device,
        mesh=split,
        in_specs=(tokens, P((*REP, "fs"), "tp"), tokens, P("fs", "tp"), P("tp", "fs")),
        out_specs=(tokens, P("fs", "tp"), P("tp", "fs")),
        check_vma=False,
    )
```

profile of v0, /device:TPU:1, one launch (start us, length us, event | category | flops | bytes accessed | tf_op | source)
XLA Modules:
  0.0 298.6 jit_solution(4348594611996614643)
XLA Ops:
  6.7 14.3 %collective-permute-done.1 = bf16[384,1024]{1,0:T(8,128)(2,1)S(1)} collective-permute-done((bf16[384,1024]{1,0:T(8,128)(2,1)S(1)}, bf16[384,1024]{1,0:T(8,128)(2,1)S(1)}, u32[]{:S(2)}, u32[]{:S(2)}) %collective-permute-start.1) | collective-permute-done | bytes 786464 | tf_op jit(solution)/shard_map/ppermute | solution.py:32
  22.9 5.4 %all-to-all-start = ((bf16[4,128,1024]{2,1,0:T(8,128)(2,1)}), bf16[4,128,1024]{2,1,0:T(8,128)(2,1)S(1)}, u32[]{:S(2)}, u32[]{:S(2)}) async-start(bf16[4,128,1024]{2,1,0:T(8,128)(2,1)} %broadcast_in_dim.18), calls=%async_computation | async-start | bytes 2097152 | tf_op jit(solution)/shard_map/all_to_all | solution.py:36
  39.9 4.4 %collective-permute-start.4 = (bf16[512,1024]{1,0:T(8,128)(2,1)S(1)}, bf16[512,1024]{1,0:T(8,128)(2,1)S(1)}, u32[]{:S(2)}, u32[]{:S(2)}) collective-permute-start(bf16[512,1024]{1,0:T(8,128)(2,1)S(1)} %bitcast.95), channel_id=1, source_target_pairs={{0,4},{1,5},{2,6},{3,7},{4,0},{5,1},{6,2},{7,3},{8,12},{9,13},{10,... | collective-permute-start | bytes 3145736 | tf_op jit(solution)/shard_map/ppermute | solution.py:32
  46.9 5.3 %collective-permute-done.3 = bf16[256,1024]{1,0:T(8,128)(2,1)} collective-permute-done((bf16[256,1024]{1,0:T(8,128)(2,1)}, bf16[256,1024]{1,0:T(8,128)(2,1)}, u32[]{:S(2)}, u32[]{:S(2)}) %collective-permute-start.3) | collective-permute-done | bytes 524320 | tf_op jit(solution)/shard_map/ppermute | solution.py:32
  55.6 7.8 %collective-permute-done.2 = bf16[256,1024]{1,0:T(8,128)(2,1)} collective-permute-done((bf16[256,1024]{1,0:T(8,128)(2,1)}, bf16[256,1024]{1,0:T(8,128)(2,1)}, u32[]{:S(2)}, u32[]{:S(2)}) %collective-permute-start.2) | collective-permute-done | bytes 524320 | tf_op jit(solution)/shard_map/ppermute | solution.py:32
  67.8 6.9 %collective-permute-start.24 = (bf16[512,2048]{1,0:T(8,128)(2,1)}, bf16[512,2048]{1,0:T(8,128)(2,1)}, u32[]{:S(2)}, u32[]{:S(2)}) collective-permute-start(bf16[512,2048]{1,0:T(8,128)(2,1)} %convolution_convert_fusion.1), channel_id=1, source_target_pairs={{0,4},{1,5},{2,6},{3,7},{4,0},{5,1},{6,2},{7,3},{8,12},{9,13},{10,... | collective-permute-start | bytes 6291464 | tf_op jit(solution)/shard_map/ppermute | solution.py:32
  83.7 4.4 %convolution_convert_fusion.2 = bf16[512,2048]{1,0:T(8,128)(2,1)} fusion(bf16[512,512]{1,0:T(8,128)(2,1)} %get-tuple-element.51, bf16[512,2048]{1,0:T(8,128)(2,1)} %copy-done.5), kind=kOutput, calls=%fused_computation.9 | convolution fusion | flops 1074790400 | bytes 4718592 | tf_op jit(solution)/shard_map/dot_general | solution.py:68
  88.1 7.2 %shard_map.79 = (bf16[2,64,2048]{2,1,0:T(8,128)(2,1)}, bf16[2,64,2048]{2,1,0:T(8,128)(2,1)}, bf16[4,64,2048]{2,1,0:T(8,128)(2,1)}) custom-call(s32[16]{0:T(128)} %stack.85.at, bf16[4,2,64,2048]{3,2,1,0:T(8,128)(2,1)} %bitcast.100, bf16[4,2,64,2048]{3,2,1,0:T(8,128)(2,1)} %bitcast.29.partner), custom_call_target="tpu_custom_call" | custom-call | flops 1048576 | bytes 6291456 | tf_op jit(solution)/shard_map/pallas_call | solution.py:101
  98.6 9.9 %collective-permute-done.25 = bf16[2,64,2048]{2,1,0:T(8,128)(2,1)S(1)} collective-permute-done((bf16[2,64,2048]{2,1,0:T(8,128)(2,1)}, bf16[2,64,2048]{2,1,0:T(8,128)(2,1)S(1)}, u32[]{:S(2)}, u32[]{:S(2)}) %collective-permute-start.25) | collective-permute-done | bytes 524320 | tf_op jit(solution)/shard_map/ppermute | solution.py:32
  120.3 7.4 %shard_map.76 = (bf16[2,256,512]{2,1,0:T(8,128)(2,1)}, bf16[2,256,512]{2,1,0:T(8,128)(2,1)}, bf16[4,256,512]{2,1,0:T(8,128)(2,1)}) custom-call(s32[16]{0:T(128)} %stack.85.at, bf16[2,4,256,512]{3,2,1,0:T(8,128)(2,1)} %bitcast.101, bf16[2,4,256,512]{3,2,1,0:T(8,128)(2,1)} %bitcast.99), custom_call_target="tpu_custom_call" | custom-call | flops 1048576 | bytes 6291456 | tf_op jit(solution)/shard_map/pallas_call | solution.py:101
  132.2 7.8 %all-to-all-start.3 = ((bf16[8,16,2048]{2,1,0:T(8,128)(2,1)}), bf16[8,16,2048]{2,1,0:T(8,128)(2,1)S(1)}, u32[]{:S(2)}, u32[]{:S(2)}) async-start(bf16[8,16,2048]{2,1,0:T(8,128)(2,1)} %bitcast.34), calls=%async_computation.3 | async-start | bytes 1048576 | tf_op jit(solution)/shard_map/all_to_all | solution.py:36
  154.6 5.0 %all-to-all-start.1 = ((bf16[8,2,32,512]{3,2,1,0:T(8,128)(2,1)}), bf16[8,2,32,512]{3,2,1,0:T(8,128)(2,1)S(1)}, u32[]{:S(2)}, u32[]{:S(2)}) async-start(bf16[8,2,32,512]{3,2,1,0:T(8,128)(2,1)} %pad_maximum_fusion.11), calls=%async_computation.1 | async-start | bytes 1048576 | tf_op jit(solution)/shard_map/all_to_all | solution.py:36
  159.7 9.3 %collective-permute-done.29 = bf16[16,1024]{1,0:T(8,128)(2,1)S(1)} collective-permute-done((bf16[16,1024]{1,0:T(8,128)(2,1)S(1)}, bf16[16,1024]{1,0:T(8,128)(2,1)S(1)}, u32[]{:S(2)}, u32[]{:S(2)}) %collective-permute-start.29) | collective-permute-done | bytes 32800 | tf_op jit(solution)/shard_map/ppermute | solution.py:32
  172.1 5.7 %all-to-all-start.4 = ((bf16[8,2,16,1024]{3,2,1,0:T(8,128)(2,1)}), bf16[8,2,16,1024]{3,2,1,0:T(8,128)(2,1)S(1)}, u32[]{:S(2)}, u32[]{:S(2)}) async-start(bf16[8,2,16,1024]{3,2,1,0:T(8,128)(2,1)} %broadcast_in_dim.42), calls=%async_computation.4 | async-start | bytes 1048576 | tf_op jit(solution)/shard_map/all_to_all | solution.py:36
  177.8 4.7 %collective-permute-start.9 = (bf16[1024,512]{1,0:T(8,128)(2,1)}, bf16[1024,512]{1,0:T(8,128)(2,1)}, u32[]{:S(2)}, u32[]{:S(2)}) collective-permute-start(bf16[1024,512]{1,0:T(8,128)(2,1)} %collective-permute-done.8), channel_id=1, source_target_pairs={{0,4},{1,5},{2,6},{3,7},{4,0},{5,1},{6,2},{7,3},{8,12},{9,13},{10,... | collective-permute-start | bytes 3145736 | tf_op jit(solution)/shard_map/ppermute | solution.py:32
  190.4 4.4 %all-to-all-start.2 = ((bf16[8,2,32,512]{3,2,1,0:T(8,128)(2,1)}), bf16[8,2,32,512]{3,2,1,0:T(8,128)(2,1)S(1)}, u32[]{:S(2)}, u32[]{:S(2)}) async-start(bf16[8,2,32,512]{3,2,1,0:T(8,128)(2,1)} %broadcast_in_dim.40), calls=%async_computation.2 | async-start | bytes 1048576 | tf_op jit(solution)/shard_map/all_to_all | solution.py:36
  201.5 5.5 %all-to-all-done.2.refs_0_ = bf16[8,2,32,512]{3,2,1,0:T(8,128)(2,1)S(1)} async-done(((bf16[8,2,32,512]{3,2,1,0:T(8,128)(2,1)}), bf16[8,2,32,512]{3,2,1,0:T(8,128)(2,1)S(1)}, u32[]{:S(2)}, u32[]{:S(2)}) %all-to-all-start.2) | async-done | bytes 524320 | tf_op jit(solution)/shard_map/all_to_all | solution.py:36
  208.8 15.3 %while.10 = (s32[]{:T(128)}, bf16[4,128,2048]{2,1,0:T(8,128)(2,1)S(1)}, bf16[4,128,1024]{2,1,0:T(8,128)(2,1)}, bf16[2048,1024]{1,0:T(8,128)(2,1)}, s32[]{:T(128)}) while((s32[]{:T(128)}, bf16[4,128,2048]{2,1,0:T(8,128)(2,1)S(1)}, bf16[4,128,1024]{2,1,0:T(8,128)(2,1)}, bf16[2048,1024]{1,0:T(8,128)(2,1)}, s32[]{:T(128)}) %tuple.49), condition=%wide.region_1.2_spmd, body=%wide.region_0.1_spmd.sunk | while | flops 537133056 | bytes 4981829 | solution.py:259
  225.5 8.0 %collective-permute-start.34 = (bf16[3,8,2,16,1024]{4,3,2,1,0:T(8,128)(2,1)S(1)}, bf16[3,8,2,16,1024]{4,3,2,1,0:T(8,128)(2,1)}, u32[]{:S(2)}, u32[]{:S(2)}) collective-permute-start(bf16[3,8,2,16,1024]{4,3,2,1,0:T(8,128)(2,1)S(1)} %pad_maximum_fusion.7), channel_id=1, source_target_pairs={{0,4},{1,5},{2,6},{3,7},{4,0},{5,1},{6,2},{7,3},{8,12},{9,13},{10,... | collective-permute-start | bytes 4718600 | tf_op jit(solution)/shard_map/ppermute | solution.py:32
  242.3 7.2 %collective-permute-done.10 = bf16[256,1024]{1,0:T(8,128)(2,1)S(1)} collective-permute-done((bf16[256,1024]{1,0:T(8,128)(2,1)S(1)}, bf16[256,1024]{1,0:T(8,128)(2,1)S(1)}, u32[]{:S(2)}, u32[]{:S(2)}) %collective-permute-start.10) | collective-permute-done | bytes 524320 | tf_op jit(solution)/shard_map/ppermute | solution.py:32
  251.1 12.5 %collective-permute-done.12 = bf16[256,1024]{1,0:T(8,128)(2,1)S(1)} collective-permute-done((bf16[256,1024]{1,0:T(8,128)(2,1)S(1)}, bf16[256,1024]{1,0:T(8,128)(2,1)S(1)}, u32[]{:S(2)}, u32[]{:S(2)}) %collective-permute-start.12) | collective-permute-done | bytes 524320 | tf_op jit(solution)/shard_map/ppermute | solution.py:32
  269.1 7.9 %collective-permute-done.11 = bf16[256,1024]{1,0:T(8,128)(2,1)S(1)} collective-permute-done((bf16[256,1024]{1,0:T(8,128)(2,1)S(1)}, bf16[256,1024]{1,0:T(8,128)(2,1)S(1)}, u32[]{:S(2)}, u32[]{:S(2)}) %collective-permute-start.11) | collective-permute-done | bytes 524320 | tf_op jit(solution)/shard_map/ppermute | solution.py:32
  278.1 6.1 %shard_map.80.refs_2_ = f32[2,2,4,128,1024]{4,3,2,1,0:T(8,128)} custom-call(s32[4]{0:T(128)} %pad_add_fusion.1.at, bf16[8,2,16,1024]{3,2,1,0:T(8,128)(2,1)} %copy-done, bf16[8,2,16,1024]{3,2,1,0:T(8,128)(2,1)} %collective-permute-done.32.refs_1_, bf16[8,2,16,1024]{3,2,1,0:T(8,128)(2,1)} %collective-permute-done.33.refs_2_, ...), custom_call_target="tpu_custom_call" | custom-call | flops 1572864 | bytes 9437184 | tf_op jit(solution)/shard_map/pallas_call | solution.py:152
  287.9 6.1 %shard_map.77.refs_2_ = f32[1024,2048]{1,0:T(8,128)} custom-call(s32[4]{0:T(128)} %pad_add_fusion.1.at, bf16[8,2,32,512]{3,2,1,0:T(8,128)(2,1)} %copy-done.1, bf16[8,2,32,512]{3,2,1,0:T(8,128)(2,1)} %collective-permute-done.21.refs_1_, bf16[8,2,32,512]{3,2,1,0:T(8,128)(2,1)} %collective-permute-done.22.refs_2_, ...), custom_call_target="tpu_custom_call" | custom-call | flops 1572864 | bytes 9437184 | tf_op jit(solution)/shard_map/pallas_call | solution.py:152
  (150 shorter events, 134.3 us)
Async XLA Ops:
  2.8 18.1 %collective-permute-start.1 = (bf16[384,1024]{1,0:T(8,128)(2,1)S(1)}, bf16[384,1024]{1,0:T(8,128)(2,1)S(1)}, u32[]{:S(2)}, u32[]{:S(2)}) collective-permute-start(bf16[384,1024]{1,0:T(8,128)(2,1)S(1)} %pad_maximum_fusion.8), channel_id=1, source_target_pairs={{0,2},{1,3},{2,0},{3,1},{4,6},{5,7},{6,4},{7,5},{8,10},{9,11},{10,... | collective-permute-start | bytes 2359304 | tf_op jit(solution)/shard_map/ppermute | solution.py:32
  6.6 29.4 %collective-permute-start = (bf16[256,1024]{1,0:T(8,128)(2,1)}, bf16[256,1024]{1,0:T(8,128)(2,1)}, u32[]{:S(2)}, u32[]{:S(2)}) collective-permute-start(bf16[256,1024]{1,0:T(8,128)(2,1)} %pad_maximum_fusion.9), channel_id=1, source_target_pairs={{0,2},{1,3},{2,0},{3,1},{4,6},{5,7},{6,4},{7,5},{8,10},{9,11},{10,... | collective-permute-start | bytes 1572872 | tf_op jit(solution)/shard_map/ppermute | solution.py:32
  28.3 23.9 %collective-permute-start.3 = (bf16[256,1024]{1,0:T(8,128)(2,1)}, bf16[256,1024]{1,0:T(8,128)(2,1)}, u32[]{:S(2)}, u32[]{:S(2)}) collective-permute-start(bf16[256,1024]{1,0:T(8,128)(2,1)} %param.9), channel_id=1, source_target_pairs={{0,3},{1,2},{2,1},{3,0},{4,7},{5,6},{6,5},{7,4},{8,11},{9,10},{10,... | collective-permute-start | bytes 1572872 | tf_op jit(solution)/shard_map/ppermute | solution.py:32
  30.8 47.7 %collective-permute-start.6 = (bf16[256,1024]{1,0:T(8,128)(2,1)}, bf16[256,1024]{1,0:T(8,128)(2,1)}, u32[]{:S(2)}, u32[]{:S(2)}) collective-permute-start(bf16[256,1024]{1,0:T(8,128)(2,1)} %param.7), channel_id=1, source_target_pairs={{0,1},{1,0},{2,3},{3,2},{4,5},{5,4},{6,7},{7,6},{8,9},{9,8},{10,11... | collective-permute-start | bytes 1572872 | tf_op jit(solution)/shard_map/ppermute | solution.py:32
  31.3 47.2 %collective-permute-start.5 = (bf16[256,1024]{1,0:T(8,128)(2,1)}, bf16[256,1024]{1,0:T(8,128)(2,1)}, u32[]{:S(2)}, u32[]{:S(2)}) collective-permute-start(bf16[256,1024]{1,0:T(8,128)(2,1)} %param.7), channel_id=1, source_target_pairs={{0,2},{1,3},{2,0},{3,1},{4,6},{5,7},{6,4},{7,5},{8,10},{9,11},{10,... | collective-permute-start | bytes 1572872 | tf_op jit(solution)/shard_map/ppermute | solution.py:32
  33.4 30.0 %collective-permute-start.2 = (bf16[256,1024]{1,0:T(8,128)(2,1)}, bf16[256,1024]{1,0:T(8,128)(2,1)}, u32[]{:S(2)}, u32[]{:S(2)}) collective-permute-start(bf16[256,1024]{1,0:T(8,128)(2,1)} %slice.187), channel_id=1, source_target_pairs={{0,3},{1,2},{2,1},{3,0},{4,7},{5,6},{6,5},{7,4},{8,11},{9,10},{10,... | collective-permute-start | bytes 1572872 | tf_op jit(solution)/shard_map/ppermute | solution.py:32
  39.9 34.8 %collective-permute-start.4 = (bf16[512,1024]{1,0:T(8,128)(2,1)S(1)}, bf16[512,1024]{1,0:T(8,128)(2,1)S(1)}, u32[]{:S(2)}, u32[]{:S(2)}) collective-permute-start(bf16[512,1024]{1,0:T(8,128)(2,1)S(1)} %bitcast.95), channel_id=1, source_target_pairs={{0,4},{1,5},{2,6},{3,7},{4,0},{5,1},{6,2},{7,3},{8,12},{9,13},{10,... | collective-permute-start | bytes 3145736 | tf_op jit(solution)/shard_map/ppermute | solution.py:32
  52.2 26.3 %collective-permute-start.7 = (bf16[256,1024]{1,0:T(8,128)(2,1)}, bf16[256,1024]{1,0:T(8,128)(2,1)S(1)}, u32[]{:S(2)}, u32[]{:S(2)}) collective-permute-start(bf16[256,1024]{1,0:T(8,128)(2,1)} %param.7), channel_id=1, source_target_pairs={{0,3},{1,2},{2,1},{3,0},{4,7},{5,6},{6,5},{7,4},{8,11},{9,10},{10,... | collective-permute-start | bytes 1572872 | tf_op jit(solution)/shard_map/ppermute | solution.py:32
  67.8 20.3 %collective-permute-start.24 = (bf16[512,2048]{1,0:T(8,128)(2,1)}, bf16[512,2048]{1,0:T(8,128)(2,1)}, u32[]{:S(2)}, u32[]{:S(2)}) collective-permute-start(bf16[512,2048]{1,0:T(8,128)(2,1)} %convolution_convert_fusion.1), channel_id=1, source_target_pairs={{0,4},{1,5},{2,6},{3,7},{4,0},{5,1},{6,2},{7,3},{8,12},{9,13},{10,... | collective-permute-start | bytes 6291464 | tf_op jit(solution)/shard_map/ppermute | solution.py:32
  83.1 35.9 %collective-permute-start.13 = (bf16[2048,512]{1,0:T(8,128)(2,1)}, bf16[2048,512]{1,0:T(8,128)(2,1)S(1)}, u32[]{:S(2)}, u32[]{:S(2)}) collective-permute-start(bf16[2048,512]{1,0:T(8,128)(2,1)} %convolution_convert_fusion.3), channel_id=1, source_target_pairs={{0,4},{1,5},{2,6},{3,7},{4,0},{5,1},{6,2},{7,3},{8,12},{9,13},{10,... | collective-permute-start | bytes 6291464 | tf_op jit(solution)/shard_map/ppermute | solution.py:32
  132.2 22.3 %all-to-all-start.3 = ((bf16[8,16,2048]{2,1,0:T(8,128)(2,1)}), bf16[8,16,2048]{2,1,0:T(8,128)(2,1)S(1)}, u32[]{:S(2)}, u32[]{:S(2)}) async-start(bf16[8,16,2048]{2,1,0:T(8,128)(2,1)} %bitcast.34), calls=%async_computation.3 | async-start | bytes 1048576 | tf_op jit(solution)/shard_map/all_to_all | solution.py:36
  147.0 30.9 %collective-permute-start.8 = (bf16[1024,512]{1,0:T(8,128)(2,1)}, bf16[1024,512]{1,0:T(8,128)(2,1)}, u32[]{:S(2)}, u32[]{:S(2)}) collective-permute-start(bf16[1024,512]{1,0:T(8,128)(2,1)} %get-tuple-element.65), channel_id=1, source_target_pairs={{0,2},{1,3},{2,0},{3,1},{4,6},{5,7},{6,4},{7,5},{8,10},{9,11},{10,... | collective-permute-start | bytes 3145736 | tf_op jit(solution)/shard_map/ppermute | solution.py:32
  172.1 17.4 %all-to-all-start.4 = ((bf16[8,2,16,1024]{3,2,1,0:T(8,128)(2,1)}), bf16[8,2,16,1024]{3,2,1,0:T(8,128)(2,1)S(1)}, u32[]{:S(2)}, u32[]{:S(2)}) async-start(bf16[8,2,16,1024]{3,2,1,0:T(8,128)(2,1)} %broadcast_in_dim.42), calls=%async_computation.4 | async-start | bytes 1048576 | tf_op jit(solution)/shard_map/all_to_all | solution.py:36
  177.8 17.2 %collective-permute-start.9 = (bf16[1024,512]{1,0:T(8,128)(2,1)}, bf16[1024,512]{1,0:T(8,128)(2,1)}, u32[]{:S(2)}, u32[]{:S(2)}) collective-permute-start(bf16[1024,512]{1,0:T(8,128)(2,1)} %collective-permute-done.8), channel_id=1, source_target_pairs={{0,4},{1,5},{2,6},{3,7},{4,0},{5,1},{6,2},{7,3},{8,12},{9,13},{10,... | collective-permute-start | bytes 3145736 | tf_op jit(solution)/shard_map/ppermute | solution.py:32
  199.4 24.8 %collective-permute-start.33 = (bf16[8,2,16,1024]{3,2,1,0:T(8,128)(2,1)S(1)}, bf16[8,2,16,1024]{3,2,1,0:T(8,128)(2,1)}, u32[]{:S(2)}, u32[]{:S(2)}) collective-permute-start(bf16[8,2,16,1024]{3,2,1,0:T(8,128)(2,1)S(1)} %all-to-all-done.4.refs_0_), channel_id=1, source_target_pairs={{0,24},{1,25},{2,26},{3,27},{4,28},{5,29},{6,30},{7,31},{8,16},{9,... | collective-permute-start | bytes 1572872 | tf_op jit(solution)/shard_map/ppermute | solution.py:32
  201.1 23.0 %collective-permute-start.32 = (bf16[8,2,16,1024]{3,2,1,0:T(8,128)(2,1)S(1)}, bf16[8,2,16,1024]{3,2,1,0:T(8,128)(2,1)}, u32[]{:S(2)}, u32[]{:S(2)}) collective-permute-start(bf16[8,2,16,1024]{3,2,1,0:T(8,128)(2,1)S(1)} %all-to-all-done.4.refs_0_), channel_id=1, source_target_pairs={{0,8},{1,9},{2,10},{3,11},{4,12},{5,13},{6,14},{7,15},{8,0},{9,1},... | collective-permute-start | bytes 1572872 | tf_op jit(solution)/shard_map/ppermute | solution.py:32
  207.0 26.5 %collective-permute-start.22 = (bf16[8,2,32,512]{3,2,1,0:T(8,128)(2,1)S(1)}, bf16[8,2,32,512]{3,2,1,0:T(8,128)(2,1)}, u32[]{:S(2)}, u32[]{:S(2)}) collective-permute-start(bf16[8,2,32,512]{3,2,1,0:T(8,128)(2,1)S(1)} %all-to-all-done.2.refs_0_), channel_id=1, source_target_pairs={{0,24},{1,25},{2,26},{3,27},{4,28},{5,29},{6,30},{7,31},{8,16},{9,... | collective-permute-start | bytes 1572872 | tf_op jit(solution)/shard_map/ppermute | solution.py:32
  208.8 24.7 %collective-permute-start.21 = (bf16[8,2,32,512]{3,2,1,0:T(8,128)(2,1)S(1)}, bf16[8,2,32,512]{3,2,1,0:T(8,128)(2,1)}, u32[]{:S(2)}, u32[]{:S(2)}) collective-permute-start(bf16[8,2,32,512]{3,2,1,0:T(8,128)(2,1)S(1)} %all-to-all-done.2.refs_0_), channel_id=1, source_target_pairs={{0,8},{1,9},{2,10},{3,11},{4,12},{5,13},{6,14},{7,15},{8,0},{9,1},... | collective-permute-start | bytes 1572872 | tf_op jit(solution)/shard_map/ppermute | solution.py:32
  225.5 52.6 %collective-permute-start.34 = (bf16[3,8,2,16,1024]{4,3,2,1,0:T(8,128)(2,1)S(1)}, bf16[3,8,2,16,1024]{4,3,2,1,0:T(8,128)(2,1)}, u32[]{:S(2)}, u32[]{:S(2)}) collective-permute-start(bf16[3,8,2,16,1024]{4,3,2,1,0:T(8,128)(2,1)S(1)} %pad_maximum_fusion.7), channel_id=1, source_target_pairs={{0,4},{1,5},{2,6},{3,7},{4,0},{5,1},{6,2},{7,3},{8,12},{9,13},{10,... | collective-permute-start | bytes 4718600 | tf_op jit(solution)/shard_map/ppermute | solution.py:32
  236.0 51.9 %collective-permute-start.23 = (bf16[3,8,2,32,512]{4,3,2,1,0:T(8,128)(2,1)}, bf16[3,8,2,32,512]{4,3,2,1,0:T(8,128)(2,1)}, u32[]{:S(2)}, u32[]{:S(2)}) collective-permute-start(bf16[3,8,2,32,512]{4,3,2,1,0:T(8,128)(2,1)} %pad_maximum_fusion.6), channel_id=1, source_target_pairs={{0,4},{1,5},{2,6},{3,7},{4,0},{5,1},{6,2},{7,3},{8,12},{9,13},{10,... | collective-permute-start | bytes 4718600 | tf_op jit(solution)/shard_map/ppermute | solution.py:32
  236.3 27.2 %collective-permute-start.12 = (bf16[256,1024]{1,0:T(8,128)(2,1)S(1)}, bf16[256,1024]{1,0:T(8,128)(2,1)S(1)}, u32[]{:S(2)}, u32[]{:S(2)}) collective-permute-start(bf16[256,1024]{1,0:T(8,128)(2,1)S(1)} %get-tuple-element.72), channel_id=1, source_target_pairs={{0,1},{1,0},{2,3},{3,2},{4,5},{5,4},{6,7},{7,6},{8,9},{9,8},{10,11... | collective-permute-start | bytes 1572872 | tf_op jit(solution)/shard_map/ppermute | solution.py:32
  240.6 22.9 %collective-permute-start.30 = (bf16[8,2,16,1024]{3,2,1,0:T(8,128)(2,1)S(1)}, bf16[8,2,16,1024]{3,2,1,0:T(8,128)(2,1)}, u32[]{:S(2)}, u32[]{:S(2)}) collective-permute-start(bf16[8,2,16,1024]{3,2,1,0:T(8,128)(2,1)S(1)} %all-to-all-done.4.refs_0_), channel_id=1, source_target_pairs={{0,16},{1,17},{2,18},{3,19},{4,20},{5,21},{6,22},{7,23},{8,24},{9,... | collective-permute-start | bytes 1572872 | tf_op jit(solution)/shard_map/ppermute | solution.py:32
  263.5 20.7 %collective-permute-start.31 = (bf16[8,2,16,1024]{3,2,1,0:T(8,128)(2,1)}, bf16[8,2,16,1024]{3,2,1,0:T(8,128)(2,1)}, u32[]{:S(2)}, u32[]{:S(2)}) collective-permute-start(bf16[8,2,16,1024]{3,2,1,0:T(8,128)(2,1)} %collective-permute-done.30.refs_0_), channel_id=1, source_target_pairs={{0,4},{1,5},{2,6},{3,7},{4,0},{5,1},{6,2},{7,3},{8,12},{9,13},{10,... | collective-permute-start | bytes 1572872 | tf_op jit(solution)/shard_map/ppermute | solution.py:32
  265.9 28.1 %collective-permute-start.20 = (bf16[8,2,32,512]{3,2,1,0:T(8,128)(2,1)}, bf16[8,2,32,512]{3,2,1,0:T(8,128)(2,1)S(1)}, u32[]{:S(2)}, u32[]{:S(2)}) collective-permute-start(bf16[8,2,32,512]{3,2,1,0:T(8,128)(2,1)} %collective-permute-done.19.refs_0_), channel_id=1, source_target_pairs={{0,4},{1,5},{2,6},{3,7},{4,0},{5,1},{6,2},{7,3},{8,12},{9,13},{10,... | collective-permute-start | bytes 1572872 | tf_op jit(solution)/shard_map/ppermute | solution.py:32
  (33 other events, 401.6 us)
where the time goes:
time: 300 us; the launch traced here: 299 us
  waiting for transfers between devices  101 us (34%)
  starting transfers between devices  87.1 us (29%)
  Pallas kernels  34.2 us (11%)
  matrix products  31.5 us (10%)
  other arithmetic  29.8 us (10%)
  local copies, waits for them, and re-layouts  14.2 us (5%)
    ppermute x35, waiting for transfers between devices, send(): return lax.ppermute(value, AXES, pairs)  84.7 us
    ppermute x35, starting transfers between devices, send(): return lax.ppermute(value, AXES, pairs)  58.8 us
    all_to_all x5, starting transfers between devices, exchange(): return lax.all_to_all(value, axis, 0, 0, tiled=True)  28.3 us
    pallas_call x4, Pallas kernels, laid(): pl.pallas_call(kernel, grid_spec=pltpu.PrefetchScalarGridSpec(num_scalar_...  19.6 us
    dot_general x5, matrix products, contract_cols(): lax.dot_general(left, right, (((1,), (1,)), ((), ())), preferred_element_...  17.6 us
    all_to_all x5, waiting for transfers between devices, exchange(): return lax.all_to_all(value, axis, 0, 0, tiled=True)  16 us
    pallas_call x2, Pallas kernels, chunk_sums(): pl.pallas_call(kernel, grid_spec=pltpu.PrefetchScalarGridSpec(num_scalar_...  14.6 us
    dot_general x4, matrix products, contract_rows(): lax.dot_general(left, right, (((0,), (0,)), ((), ())), preferred_element_...  13.9 us
  transfers between devices with their start and end apart: 40, of which 18 were waited for; matrix products, arithmetic and copies ran while one was open for 24% of the time, Pallas kernels for 10%

commit v1 on v0

--- a/solution.py
+++ b/solution.py
@@ -74,41 +74,6 @@
 
 def tokens_of(own, near, far, diag):
     return jnp.concatenate([jnp.concatenate([own, near], 1), jnp.concatenate([far, diag], 1)], 0)
-
-
-CHUNKS = ((2, 0), (1, 0), (2, 1), (3, 1), (1, 1), (3, 0), (0, 0), (0, 1))
-
-
-def chunk_sums(y, own, partner, halves_first):
-    rows, columns = own.shape[2:]
-    at = jnp.stack([part for flip, half in CHUNKS for part in (y ^ flip, half)]).astype(jnp.int32)
-
-    def kernel(at, own, partner, one, three, rest):
-        total = (own[0].astype(jnp.float32) + partner[0].astype(jnp.float32)).astype(jnp.bfloat16)
-        step = pl.program_id(0)
-        for target, low, high in ((one, 0, 2), (three, 2, 4), (rest, 4, 8)):
-
-            @pl.when((step >= low) & (step < high))
-            def _(target=target):
-                target[...] = total
-
-    def source(i, at):
-        return (at[2 * i + 1], at[2 * i], 0, 0) if halves_first else (at[2 * i], at[2 * i + 1], 0, 0)
-
-    def target(low, high):
-        return pl.BlockSpec((1, rows, columns), lambda i, at: (jnp.clip(i - low, 0, high - low - 1), 0, 0))
-
-    return pl.pallas_call(
-        kernel,
-        grid_spec=pltpu.PrefetchScalarGridSpec(
-            num_scalar_prefetch=1,
-            grid=(len(CHUNKS),),
-            in_specs=[pl.BlockSpec((1, 1, rows, columns), source)] * 2,
-            out_specs=[target(0, 2), target(2, 4), target(4, 8)],
-        ),
-        out_shape=[jax.ShapeDtypeStruct((n, rows, columns), jnp.bfloat16) for n in (2, 2, 4)],
-        cost_estimate=pl.CostEstimate(flops=own.size, bytes_accessed=own.size * 6, transcendentals=0),
-    )(at, own, partner)
 
 
 def laid(out, group, c, shape, by_rows, scale):
@@ -178,9 +143,8 @@
     def cols_by_core(value, start):
         return jnp.concatenate([cols_of(value, start + first, eighth), cols_of(value, start + second, eighth)], 1)
 
-    down_near = rows_of(down_weight, theirs + first + y * (eighth // NY), eighth // NY)
-    cot_near = send(jnp.concatenate([cotangent, down_near]), fs=1)
-    cot_near, down_near = fixed((cot_near[:rows], cot_near[rows:]))
+    down_near = send(rows_of(down_weight, theirs + first + y * (eighth // NY), eighth // NY), fs=1)
+    cot_near = send(cotangent, fs=1)
     cot_diag = send(cotangent, fs=1, tp=1)
     pre_near = send(cols_by_core(pre_act, theirs), fs=1)
     down_near = to_all(down_near, "y").reshape(eighth, half_d)
@@ -189,8 +153,7 @@
     in_near = send(inputs, fs=1)
     in_diag = send(inputs, fs=1, tp=1)
     in_far = send(inputs, tp=1)
-    up_near = send(cols_of(up_weight, theirs + first, eighth), fs=1)
-    up_other = send(up_near, c=1)
+    up_near = send(cols_by_core(up_weight, theirs), fs=1)
 
     down_own = fixed(
         jnp.concatenate(
@@ -206,58 +169,63 @@
     down_part = contract_rows(square[0], cot).astype(jnp.bfloat16)
     down_parts = (down_part, send(contract_rows(square[1], cot).astype(jnp.bfloat16), c=1))
 
-    split = (NY, 2, eighth // NY // 2, 2 * half_d)
-    down_sums = chunk_sums(y, *[part.reshape(split) for part in down_parts], False)
-
+    down_sums = fixed(
+        tuple(
+            added(*[rows_of(part, (y ^ flip) * (eighth // NY), eighth // NY) for part in down_parts])
+            for flip in (1, 3, 2, 0)
+        )
+    )
     down = fixed(jnp.concatenate([down_own, fixed(jnp.concatenate([down_near, down_other]))], 1))
     grad_pre = fixed((2.0 * positive * contract_cols(cot, down)).astype(jnp.bfloat16))
-    grad_pre, *ready = fixed((grad_pre, inputs, in_near, in_far, in_diag, down_sums[0][0, :1]))[:5]
+    grad_pre, *ready = fixed((grad_pre, inputs, in_near, in_far, in_diag, down_sums[3][:1]))[:5]
     x = fixed(tokens_of(*ready))
-    up_parts = tuple(
-        contract_rows(x, g).astype(jnp.bfloat16) for g in (grad_pre[:, :eighth], grad_pre[:, eighth:])
-    )
-    up_parts = (up_parts[0], send(up_parts[1], c=1))
-
-    split = (2, NY, half_d // NY, eighth)
-    up_sums = chunk_sums(y, *[part.reshape(split) for part in up_parts], True)
-
-    def y_sum(one, three, rest):
-        one = send(one, y=1)
-        three = send(three, y=3)
-        right = send(added(rest[0], three[0]), y=1)
-        left = send(added(rest[1], one[0]), y=3)
-        return added(rest[2], one[1], left), added(rest[3], three[1], right)
+    up_part = contract_rows(x, grad_pre[:, :eighth]).astype(jnp.bfloat16)
+    up_parts = (
+        up_part,
+        send(contract_rows(x, grad_pre[:, eighth:]).astype(jnp.bfloat16), c=1),
+    )
+    up_parts = [part.reshape(2, NY * nz * rows_up, eighth) for part in up_parts]
+    size = nz * rows_up
+    up_sums = fixed(
+        tuple(
+            added(*[lax.dynamic_slice_in_dim(part, (y ^ flip) * size, size, axis=1) for part in up_parts])
+            for flip in (1, 3, 2, 0)
+        )
+    )
+
+    def y_sum(one, three, two, own):
+        got = send(one, y=1), send(three, y=3), send(two, y=2)
+        return added(own, *got)
 
     def z_sum(value):
         got = exchange(value, "z")
         return added(*[got[i] for i in range(nz)])
 
-    def gathered(own, other):
+    def gathered(own, other, cut):
         both = jnp.stack(ordered(fs == 1, own, send(other, fs=1)))
         value = to_all(both, "z").reshape(nz, *both.shape)
         ways = ((y ^ 1, 1), (y ^ 3, 3), (y ^ 2, 2))
         found = [(y, value)] + [(at, send(value, y=flip)) for at, flip in ways]
-        near, far = [v for _, v in found[:3]], found[3][1]
-        passed = send(jnp.stack(near), c=1)
         places = jnp.stack([at for at, _ in found])
-        return (places[:3], near, passed), (places[3:], [far], send(far, c=1)[None])
-
-    d = jnp.concatenate(y_sum(*down_sums)).reshape(nz, rows_down, 2 * half_d)
-    d = z_sum(d)
-    u = jnp.stack([half.reshape(nz, rows_up, eighth) for half in y_sum(*up_sums)], 1)
+        values = [v for _, v in found]
+        near = jnp.stack(values[:3] if cut else values)
+        passed = send(near, c=1)
+        if not cut:
+            return ((places, values, passed),)
+        return (places[:3], values[:3], passed), (places[3:], values[3:], send(values[3], c=1)[None])
+
+    d = z_sum(y_sum(*down_sums).reshape(nz, rows_down, 2 * half_d))
+    u = y_sum(*up_sums).reshape(2, nz, rows_up, eighth).transpose(1, 0, 2, 3)
     u = z_sum(u)
-    near, far = gathered(d[:, :half_d], d[:, half_d:])
+    (group,) = gathered(d[:, :half_d], d[:, half_d:], False)
     shape = (2, NC, NY, nz * rows_down, half_d)
-    grad_down = laid(None, near, c, shape, True, factor)
-    grad_down = laid(grad_down, far, c, shape, True, factor)
-    near, far = gathered(u[0], u[1])
+    grad_down = laid(None, group, c, shape, True, factor)
+    near, far = gathered(u[0], u[1], True)
     grad_up = laid(None, near, c, (half_d, width), False, factor)
     grad_up = laid(grad_up, far, c, (half_d, width), False, factor)
 
-    up_own = fixed(cols_by_core(up_weight, mine))
-    up = fixed(jnp.concatenate([up_own, fixed(jnp.concatenate([up_near, up_other], 1))]))
-    part = lax.map(lambda r: contract_cols(r, up).astype(jnp.bfloat16), grad_pre.reshape(4, rows // 2, quarter))
-    part = part.reshape(2 * rows, 2 * half_d)
+    up = fixed(jnp.concatenate([fixed(cols_by_core(up_weight, mine)), up_near]))
+    part = contract_cols(grad_pre, up).astype(jnp.bfloat16)
     grad_inputs = ring_sum(
         part[:rows, :half_d],
         part[:rows, half_d:],

time: 300 us -> 338 us (1.13)
  waiting for transfers between devices: 101 us -> 168 us
  Pallas kernels: 34.2 us -> 17.3 us
  matrix products: 31.5 us -> 19.7 us
  starting transfers between devices: 87.1 us -> 81.8 us
  other arithmetic: 29.8 us -> 34.7 us
    ppermute x35 -> x32, waiting for transfers between devices: 84.7 us -> 156 us  [send(): return lax.ppermute(value, AXES, pairs)]
    pallas_call x2 -> x0, Pallas kernels: 14.6 us -> none  [chunk_sums(): pl.pallas_call(kernel, grid_spec=pltpu.PrefetchScalarGridSpec(num_scalar_...]
    dot_general x5 -> x2, matrix products: 17.6 us -> 7.27 us  [contract_cols(): lax.dot_general(left, right, (((1,), (1,)), ((), ())), preferred_element_...]
    ppermute x35 -> x32, starting transfers between devices: 58.8 us -> 52.5 us  [send(): return lax.ppermute(value, AXES, pairs)]
    convert_element_type x7, other arithmetic: 7.15 us -> 13.3 us  [added(): return total.astype(jnp.bfloat16)]
    all_to_all x5, waiting for transfers between devices: 16 us -> 11.7 us  [exchange(): return lax.all_to_all(value, axis, 0, 0, tiled=True)]
    pallas_call x4 -> x3, Pallas kernels: 19.6 us -> 17.3 us  [laid(): pl.pallas_call(kernel, grid_spec=pltpu.PrefetchScalarGridSpec(num_scalar_...]
  transfers between devices with their start and end apart: 40 -> 37, of which waited for: 18 -> 19; matrix products, arithmetic and copies ran while one was open for 24% -> 20% of each run, Pallas kernels for 10% -> 4%
where the time goes in v1:
time: 338 us; the launch traced here: 337 us
  waiting for transfers between devices  168 us (50%)
  starting transfers between devices  81.8 us (24%)
  other arithmetic  34.7 us (10%)
  matrix products  19.7 us (6%)
  Pallas kernels  17.3 us (5%)
  local copies, waits for them, and re-layouts  14.5 us (4%)
    ppermute x32, waiting for transfers between devices, send(): return lax.ppermute(value, AXES, pairs)  156 us
    ppermute x32, starting transfers between devices, send(): return lax.ppermute(value, AXES, pairs)  52.5 us
    all_to_all x5, starting transfers between devices, exchange(): return lax.all_to_all(value, axis, 0, 0, tiled=True)  29.3 us
    pallas_call x3, Pallas kernels, laid(): pl.pallas_call(kernel, grid_spec=pltpu.PrefetchScalarGridSpec(num_scalar_...  17.3 us
    convert_element_type x7, other arithmetic, added(): return total.astype(jnp.bfloat16)  13.3 us
    dot_general x4, matrix products, contract_rows(): lax.dot_general(left, right, (((0,), (0,)), ((), ())), preferred_element_...  12.4 us
    all_to_all x5, waiting for transfers between devices, exchange(): return lax.all_to_all(value, axis, 0, 0, tiled=True)  11.7 us
    dot_general x2, matrix products, contract_cols(): lax.dot_general(left, right, (((1,), (1,)), ((), ())), preferred_element_...  7.27 us
  transfers between devices with their start and end apart: 37, of which 19 were waited for; matrix products, arithmetic and copies ran while one was open for 20% of the time, Pallas kernels for 4%

profile of v1, /device:TPU:1, one launch (start us, length us, event | category | flops | bytes accessed | tf_op | source)
XLA Modules:
  0.0 336.7 jit_solution(17391275120848433209)
XLA Ops:
  8.1 10.9 %collective-permute-done.4 = bf16[128,1024]{1,0:T(8,128)(2,1)S(1)} collective-permute-done((bf16[128,1024]{1,0:T(8,128)(2,1)S(1)}, bf16[128,1024]{1,0:T(8,128)(2,1)S(1)}, u32[]{:S(2)}, u32[]{:S(2)}) %collective-permute-start.4) | collective-permute-done | bytes 262176 | tf_op jit(solution)/shard_map/ppermute | solution.py:32
  20.1 5.4 %all-to-all-start = ((bf16[4,128,1024]{2,1,0:T(8,128)(2,1)}), bf16[4,128,1024]{2,1,0:T(8,128)(2,1)S(1)}, u32[]{:S(2)}, u32[]{:S(2)}) async-start(bf16[4,128,1024]{2,1,0:T(8,128)(2,1)} %broadcast_in_dim.10), calls=%async_computation | async-start | bytes 2097152 | tf_op jit(solution)/shard_map/all_to_all | solution.py:36
  36.7 4.8 %collective-permute-start.5 = (bf16[512,1024]{1,0:T(8,128)(2,1)S(1)}, bf16[512,1024]{1,0:T(8,128)(2,1)S(1)}, u32[]{:S(2)}, u32[]{:S(2)}) collective-permute-start(bf16[512,1024]{1,0:T(8,128)(2,1)S(1)} %bitcast.52), channel_id=1, source_target_pairs={{0,4},{1,5},{2,6},{3,7},{4,0},{5,1},{6,2},{7,3},{8,12},{9,13},{10,... | collective-permute-start | bytes 3145736 | tf_op jit(solution)/shard_map/ppermute | solution.py:32
  46.6 12.6 %collective-permute-done.2 = bf16[256,1024]{1,0:T(8,128)(2,1)} collective-permute-done((bf16[256,1024]{1,0:T(8,128)(2,1)}, bf16[256,1024]{1,0:T(8,128)(2,1)}, u32[]{:S(2)}, u32[]{:S(2)}) %collective-permute-start.2) | collective-permute-done | bytes 524320 | tf_op jit(solution)/shard_map/ppermute | solution.py:32
  63.5 8.9 %collective-permute-start.23 = (bf16[512,2048]{1,0:T(8,128)(2,1)}, bf16[512,2048]{1,0:T(8,128)(2,1)}, u32[]{:S(2)}, u32[]{:S(2)}) collective-permute-start(bf16[512,2048]{1,0:T(8,128)(2,1)} %convolution_convert_fusion.1), channel_id=1, source_target_pairs={{0,4},{1,5},{2,6},{3,7},{4,0},{5,1},{6,2},{7,3},{8,12},{9,13},{10,... | collective-permute-start | bytes 6291464 | tf_op jit(solution)/shard_map/ppermute | solution.py:32
  91.0 4.3 %convolution_convert_fusion.4 = bf16[2048,512]{1,0:T(8,128)(2,1)} fusion(bf16[512,2048]{1,0:T(8,128)(2,1)} %copy-done.5, bf16[512,1024]{1,0:T(8,128)(2,1)} %copy-done.18), kind=kOutput, calls=%fused_computation.6 | convolution fusion | flops 1074790400 | bytes 4718592 | tf_op jit(solution)/shard_map/dot_general | solution.py:68
  95.3 6.8 %collective-permute-done.26 = bf16[128,2048]{1,0:T(8,128)(2,1)} collective-permute-done((bf16[128,2048]{1,0:T(8,128)(2,1)}, bf16[128,2048]{1,0:T(8,128)(2,1)}, u32[]{:S(2)}, u32[]{:S(2)}) %collective-permute-start.26) | collective-permute-done | bytes 524320 | tf_op jit(solution)/shard_map/ppermute | solution.py:32
  102.1 11.9 %collective-permute-done.25 = bf16[128,2048]{1,0:T(8,128)(2,1)} collective-permute-done((bf16[128,2048]{1,0:T(8,128)(2,1)}, bf16[128,2048]{1,0:T(8,128)(2,1)}, u32[]{:S(2)}, u32[]{:S(2)}) %collective-permute-start.25) | collective-permute-done | bytes 524320 | tf_op jit(solution)/shard_map/ppermute | solution.py:32
  116.5 7.5 %all-to-all-start.3 = ((bf16[8,16,2048]{2,1,0:T(8,128)(2,1)}), bf16[8,16,2048]{2,1,0:T(8,128)(2,1)}, u32[]{:S(2)}, u32[]{:S(2)}) async-start(bf16[8,16,2048]{2,1,0:T(8,128)(2,1)} %bitcast.18), calls=%async_computation.3 | async-start | bytes 1048576 | tf_op jit(solution)/shard_map/all_to_all | solution.py:36
  131.7 8.7 %collective-permute-done.16 = bf16[2,256,512]{2,1,0:T(8,128)(2,1)S(1)} collective-permute-done((bf16[2,256,512]{2,1,0:T(8,128)(2,1)S(1)}, bf16[2,256,512]{2,1,0:T(8,128)(2,1)S(1)}, u32[]{:S(2)}, u32[]{:S(2)}) %collective-permute-start.16) | collective-permute-done | bytes 524320 | tf_op jit(solution)/shard_map/ppermute | solution.py:32
  140.4 12.5 %collective-permute-done.15 = bf16[2,256,512]{2,1,0:T(8,128)(2,1)S(1)} collective-permute-done((bf16[2,256,512]{2,1,0:T(8,128)(2,1)S(1)}, bf16[2,256,512]{2,1,0:T(8,128)(2,1)S(1)}, u32[]{:S(2)}, u32[]{:S(2)}) %collective-permute-start.15) | collective-permute-done | bytes 524320 | tf_op jit(solution)/shard_map/ppermute | solution.py:32
  154.1 6.6 %all-to-all-start.1 = ((bf16[8,2,32,512]{3,2,1,0:T(8,128)(2,1)}), bf16[8,2,32,512]{3,2,1,0:T(8,128)(2,1)}, u32[]{:S(2)}, u32[]{:S(2)}) async-start(bf16[8,2,32,512]{3,2,1,0:T(8,128)(2,1)} %copy.10), calls=%async_computation.1 | async-start | bytes 1048576 | tf_op jit(solution)/shard_map/all_to_all | solution.py:36
  166.3 44.4 %collective-permute-done.27 = bf16[16,1024]{1,0:T(8,128)(2,1)S(1)} collective-permute-done((bf16[16,1024]{1,0:T(8,128)(2,1)S(1)}, bf16[16,1024]{1,0:T(8,128)(2,1)S(1)}, u32[]{:S(2)}, u32[]{:S(2)}) %collective-permute-start.27) | collective-permute-done | bytes 32800 | tf_op jit(solution)/shard_map/ppermute | solution.py:32
  211.6 6.4 %all-to-all-start.4 = ((bf16[8,2,16,1024]{3,2,1,0:T(8,128)(2,1)}), bf16[8,2,16,1024]{3,2,1,0:T(8,128)(2,1)S(1)}, u32[]{:S(2)}, u32[]{:S(2)}) async-start(bf16[8,2,16,1024]{3,2,1,0:T(8,128)(2,1)} %broadcast_in_dim.14), calls=%async_computation.4 | async-start | bytes 1048576 | tf_op jit(solution)/shard_map/all_to_all | solution.py:36
  222.0 11.2 %all-to-all-done.4.refs_0_ = bf16[8,2,16,1024]{3,2,1,0:T(8,128)(2,1)S(1)} async-done(((bf16[8,2,16,1024]{3,2,1,0:T(8,128)(2,1)}), bf16[8,2,16,1024]{3,2,1,0:T(8,128)(2,1)S(1)}, u32[]{:S(2)}, u32[]{:S(2)}) %all-to-all-start.4) | async-done | bytes 524320 | tf_op jit(solution)/shard_map/all_to_all | solution.py:36
  242.7 4.1 %pad_maximum_fusion.1 = bf16[2048,1024]{1,0:T(8,128)(2,1)} fusion(bf16[1024,1024]{1,0:T(8,128)(2,1)} %collective-permute-done.9, bf16[1024,1024]{1,0:T(8,128)(2,1)S(1)} %pad_maximum_fusion.4), kind=kLoop, calls=%fused_computation.1 | loop fusion | flops 8388608 | bytes 8388608 | tf_op jit(solution)/shard_map/concatenate | solution.py:227
  251.7 11.3 %collective-permute-done.30.refs_3_ = bf16[8,2,16,1024]{3,2,1,0:T(8,128)(2,1)S(1)} collective-permute-done((bf16[8,2,16,1024]{3,2,1,0:T(8,128)(2,1)S(1)}, bf16[8,2,16,1024]{3,2,1,0:T(8,128)(2,1)S(1)}, u32[]{:S(2)}, u32[]{:S(2)}) %collective-permute-start.30) | collective-permute-done | bytes 524320 | tf_op jit(solution)/shard_map/ppermute | solution.py:32
  264.6 4.0 %collective-permute-start.31 = (bf16[4,8,2,16,1024]{4,3,2,1,0:T(8,128)(2,1)}, bf16[4,8,2,16,1024]{4,3,2,1,0:T(8,128)(2,1)S(1)}, u32[]{:S(2)}, u32[]{:S(2)}) collective-permute-start(bf16[4,8,2,16,1024]{4,3,2,1,0:T(8,128)(2,1)} %pad_maximum_fusion.6), channel_id=1, source_target_pairs={{0,4},{1,5},{2,6},{3,7},{4,0},{5,1},{6,2},{7,3},{8,12},{9,13},{10,... | collective-permute-start | bytes 6291464 | tf_op jit(solution)/shard_map/ppermute | solution.py:32
  270.0 4.9 %convolution_convert_fusion = bf16[512,2048]{1,0:T(8,128)(2,1)S(1)} fusion(bf16[512,1024]{1,0:T(8,128)(2,1)} %copy-done.18, bf16[2048,1024]{1,0:T(8,128)(2,1)} %pad_maximum_fusion.1), kind=kOutput, calls=%fused_computation.2 | convolution fusion | flops 2148532224 | bytes 7340032 | tf_op jit(solution)/shard_map/dot_general | solution.py:72
  274.9 7.0 %collective-permute-done.20.refs_1_ = bf16[8,2,32,512]{3,2,1,0:T(8,128)(2,1)S(1)} collective-permute-done((bf16[8,2,32,512]{3,2,1,0:T(8,128)(2,1)S(1)}, bf16[8,2,32,512]{3,2,1,0:T(8,128)(2,1)S(1)}, u32[]{:S(2)}, u32[]{:S(2)}) %collective-permute-start.20) | collective-permute-done | bytes 524320 | tf_op jit(solution)/shard_map/ppermute | solution.py:32
  290.7 11.1 %collective-permute-done.12 = bf16[256,1024]{1,0:T(8,128)(2,1)S(1)} collective-permute-done((bf16[256,1024]{1,0:T(8,128)(2,1)S(1)}, bf16[256,1024]{1,0:T(8,128)(2,1)S(1)}, u32[]{:S(2)}, u32[]{:S(2)}) %collective-permute-start.12) | collective-permute-done | bytes 524320 | tf_op jit(solution)/shard_map/ppermute | solution.py:32
  307.1 6.3 %collective-permute-done.11 = bf16[256,1024]{1,0:T(8,128)(2,1)} collective-permute-done((bf16[256,1024]{1,0:T(8,128)(2,1)}, bf16[256,1024]{1,0:T(8,128)(2,1)}, u32[]{:S(2)}, u32[]{:S(2)}) %collective-permute-start.11) | collective-permute-done | bytes 524320 | tf_op jit(solution)/shard_map/ppermute | solution.py:32
  318.6 7.5 %shard_map.78 = f32[2,2,4,128,1024]{4,3,2,1,0:T(8,128)} custom-call(s32[5]{0:T(128)} %concatenate.71.at, bf16[8,2,16,1024]{3,2,1,0:T(8,128)(2,1)} %copy-done.1, bf16[8,2,16,1024]{3,2,1,0:T(8,128)(2,1)} %copy-done.11, bf16[8,2,16,1024]{3,2,1,0:T(8,128)(2,1)} %copy-done.12, bf16[8,2,16,1024]{3,2,1,0:T(8,128)(2,1)} %copy-done.13, ...), custom_call_target="tpu_custom_call" | custom-call | flops 2097152 | bytes 12582912 | tf_op jit(solution)/shard_map/pallas_call | solution.py:117
  326.1 6.1 %shard_map.76.refs_2_ = f32[1024,2048]{1,0:T(8,128)} custom-call(s32[4]{0:T(128)} %pad_add_fusion.1.at, bf16[8,2,32,512]{3,2,1,0:T(8,128)(2,1)} %copy-done, bf16[8,2,32,512]{3,2,1,0:T(8,128)(2,1)} %copy-done.7, bf16[8,2,32,512]{3,2,1,0:T(8,128)(2,1)} %copy-done.8, bf16[3,8,2,32,512]{4,3,2,1,0:T(8,128)(2,1)} %collective-permute-done.22.refs_3_), custom_call_target="tpu_custom_call" | custom-call | flops 1572864 | bytes 9437184 | tf_op jit(solution)/shard_map/pallas_call | solution.py:117
  (136 shorter events, 110.7 us)
Async XLA Ops:
  0.6 30.6 %collective-permute-start.1 = (bf16[256,1024]{1,0:T(8,128)(2,1)}, bf16[256,1024]{1,0:T(8,128)(2,1)}, u32[]{:S(2)}, u32[]{:S(2)}) collective-permute-start(bf16[256,1024]{1,0:T(8,128)(2,1)} %param.7), channel_id=1, source_target_pairs={{0,2},{1,3},{2,0},{3,1},{4,6},{5,7},{6,4},{7,5},{8,10},{9,11},{10,... | collective-permute-start | bytes 1572872 | tf_op jit(solution)/shard_map/ppermute | solution.py:32
  6.7 27.1 %collective-permute-start = (bf16[256,1024]{1,0:T(8,128)(2,1)}, bf16[256,1024]{1,0:T(8,128)(2,1)}, u32[]{:S(2)}, u32[]{:S(2)}) collective-permute-start(bf16[256,1024]{1,0:T(8,128)(2,1)} %pad_maximum_fusion.8), channel_id=1, source_target_pairs={{0,2},{1,3},{2,0},{3,1},{4,6},{5,7},{6,4},{7,5},{8,10},{9,11},{10,... | collective-permute-start | bytes 1572872 | tf_op jit(solution)/shard_map/ppermute | solution.py:32
  27.9 48.3 %collective-permute-start.6 = (bf16[256,1024]{1,0:T(8,128)(2,1)}, bf16[256,1024]{1,0:T(8,128)(2,1)}, u32[]{:S(2)}, u32[]{:S(2)}) collective-permute-start(bf16[256,1024]{1,0:T(8,128)(2,1)} %param.5), channel_id=1, source_target_pairs={{0,2},{1,3},{2,0},{3,1},{4,6},{5,7},{6,4},{7,5},{8,10},{9,11},{10,... | collective-permute-start | bytes 1572872 | tf_op jit(solution)/shard_map/ppermute | solution.py:32
  27.9 48.3 %collective-permute-start.7 = (bf16[256,1024]{1,0:T(8,128)(2,1)}, bf16[256,1024]{1,0:T(8,128)(2,1)}, u32[]{:S(2)}, u32[]{:S(2)}) collective-permute-start(bf16[256,1024]{1,0:T(8,128)(2,1)} %param.5), channel_id=1, source_target_pairs={{0,1},{1,0},{2,3},{3,2},{4,5},{5,4},{6,7},{7,6},{8,9},{9,8},{10,11... | collective-permute-start | bytes 1572872 | tf_op jit(solution)/shard_map/ppermute | solution.py:32
  31.2 27.9 %collective-permute-start.2 = (bf16[256,1024]{1,0:T(8,128)(2,1)}, bf16[256,1024]{1,0:T(8,128)(2,1)}, u32[]{:S(2)}, u32[]{:S(2)}) collective-permute-start(bf16[256,1024]{1,0:T(8,128)(2,1)} %collective-permute-done.1), channel_id=1, source_target_pairs={{0,3},{1,2},{2,1},{3,0},{4,7},{5,6},{6,5},{7,4},{8,11},{9,10},{10,... | collective-permute-start | bytes 1572872 | tf_op jit(solution)/shard_map/ppermute | solution.py:32
  36.7 35.7 %collective-permute-start.5 = (bf16[512,1024]{1,0:T(8,128)(2,1)S(1)}, bf16[512,1024]{1,0:T(8,128)(2,1)S(1)}, u32[]{:S(2)}, u32[]{:S(2)}) collective-permute-start(bf16[512,1024]{1,0:T(8,128)(2,1)S(1)} %bitcast.52), channel_id=1, source_target_pairs={{0,4},{1,5},{2,6},{3,7},{4,0},{5,1},{6,2},{7,3},{8,12},{9,13},{10,... | collective-permute-start | bytes 3145736 | tf_op jit(solution)/shard_map/ppermute | solution.py:32
  44.1 32.1 %collective-permute-start.8 = (bf16[256,1024]{1,0:T(8,128)(2,1)}, bf16[256,1024]{1,0:T(8,128)(2,1)S(1)}, u32[]{:S(2)}, u32[]{:S(2)}) collective-permute-start(bf16[256,1024]{1,0:T(8,128)(2,1)} %param.5), channel_id=1, source_target_pairs={{0,3},{1,2},{2,1},{3,0},{4,7},{5,6},{6,5},{7,4},{8,11},{9,10},{10,... | collective-permute-start | bytes 1572872 | tf_op jit(solution)/shard_map/ppermute | solution.py:32
  63.5 20.2 %collective-permute-start.23 = (bf16[512,2048]{1,0:T(8,128)(2,1)}, bf16[512,2048]{1,0:T(8,128)(2,1)}, u32[]{:S(2)}, u32[]{:S(2)}) collective-permute-start(bf16[512,2048]{1,0:T(8,128)(2,1)} %convolution_convert_fusion.1), channel_id=1, source_target_pairs={{0,4},{1,5},{2,6},{3,7},{4,0},{5,1},{6,2},{7,3},{8,12},{9,13},{10,... | collective-permute-start | bytes 6291464 | tf_op jit(solution)/shard_map/ppermute | solution.py:32
  80.8 43.2 %collective-permute-start.13 = (bf16[2048,512]{1,0:T(8,128)(2,1)}, bf16[2048,512]{1,0:T(8,128)(2,1)S(1)}, u32[]{:S(2)}, u32[]{:S(2)}) collective-permute-start(bf16[2048,512]{1,0:T(8,128)(2,1)} %convolution_convert_fusion.3), channel_id=1, source_target_pairs={{0,4},{1,5},{2,6},{3,7},{4,0},{5,1},{6,2},{7,3},{8,12},{9,13},{10,... | collective-permute-start | bytes 6291464 | tf_op jit(solution)/shard_map/ppermute | solution.py:32
  90.1 23.9 %collective-permute-start.25 = (bf16[128,2048]{1,0:T(8,128)(2,1)}, bf16[128,2048]{1,0:T(8,128)(2,1)}, u32[]{:S(2)}, u32[]{:S(2)}) collective-permute-start(bf16[128,2048]{1,0:T(8,128)(2,1)} %get-tuple-element.31), channel_id=1, source_target_pairs={{0,24},{1,25},{2,26},{3,27},{4,28},{5,29},{6,30},{7,31},{8,16},{9,... | collective-permute-start | bytes 1572872 | tf_op jit(solution)/shard_map/ppermute | solution.py:32
  91.0 23.0 %collective-permute-start.24 = (bf16[128,2048]{1,0:T(8,128)(2,1)S(1)}, bf16[128,2048]{1,0:T(8,128)(2,1)}, u32[]{:S(2)}, u32[]{:S(2)}) collective-permute-start(bf16[128,2048]{1,0:T(8,128)(2,1)S(1)} %get-tuple-element.30), channel_id=1, source_target_pairs={{0,8},{1,9},{2,10},{3,11},{4,12},{5,13},{6,14},{7,15},{8,0},{9,1},... | collective-permute-start | bytes 1572872 | tf_op jit(solution)/shard_map/ppermute | solution.py:32
  116.5 37.6 %all-to-all-start.3 = ((bf16[8,16,2048]{2,1,0:T(8,128)(2,1)}), bf16[8,16,2048]{2,1,0:T(8,128)(2,1)}, u32[]{:S(2)}, u32[]{:S(2)}) async-start(bf16[8,16,2048]{2,1,0:T(8,128)(2,1)} %bitcast.18), calls=%async_computation.3 | async-start | bytes 1048576 | tf_op jit(solution)/shard_map/all_to_all | solution.py:36
  127.6 25.3 %collective-permute-start.15 = (bf16[2,256,512]{2,1,0:T(8,128)(2,1)S(1)}, bf16[2,256,512]{2,1,0:T(8,128)(2,1)S(1)}, u32[]{:S(2)}, u32[]{:S(2)}) collective-permute-start(bf16[2,256,512]{2,1,0:T(8,128)(2,1)S(1)} %get-tuple-element.25), channel_id=1, source_target_pairs={{0,24},{1,25},{2,26},{3,27},{4,28},{5,29},{6,30},{7,31},{8,16},{9,... | collective-permute-start | bytes 1572872 | tf_op jit(solution)/shard_map/ppermute | solution.py:32
  130.2 22.7 %collective-permute-start.14 = (bf16[2,256,512]{2,1,0:T(8,128)(2,1)S(1)}, bf16[2,256,512]{2,1,0:T(8,128)(2,1)S(1)}, u32[]{:S(2)}, u32[]{:S(2)}) collective-permute-start(bf16[2,256,512]{2,1,0:T(8,128)(2,1)S(1)} %get-tuple-element.24), channel_id=1, source_target_pairs={{0,8},{1,9},{2,10},{3,11},{4,12},{5,13},{6,14},{7,15},{8,0},{9,1},... | collective-permute-start | bytes 1572872 | tf_op jit(solution)/shard_map/ppermute | solution.py:32
  154.1 56.6 %all-to-all-start.1 = ((bf16[8,2,32,512]{3,2,1,0:T(8,128)(2,1)}), bf16[8,2,32,512]{3,2,1,0:T(8,128)(2,1)}, u32[]{:S(2)}, u32[]{:S(2)}) async-start(bf16[8,2,32,512]{3,2,1,0:T(8,128)(2,1)} %copy.10), calls=%async_computation.1 | async-start | bytes 1048576 | tf_op jit(solution)/shard_map/all_to_all | solution.py:36
  163.6 79.1 %collective-permute-start.9 = (bf16[1024,1024]{1,0:T(8,128)(2,1)}, bf16[1024,1024]{1,0:T(8,128)(2,1)}, u32[]{:S(2)}, u32[]{:S(2)}) collective-permute-start(bf16[1024,1024]{1,0:T(8,128)(2,1)} %pad_maximum_fusion.5), channel_id=1, source_target_pairs={{0,2},{1,3},{2,0},{3,1},{4,6},{5,7},{6,4},{7,5},{8,10},{9,11},{10,... | collective-permute-start | bytes 6291464 | tf_op jit(solution)/shard_map/ppermute | solution.py:32
  164.7 46.0 %collective-permute-start.27 = (bf16[16,1024]{1,0:T(8,128)(2,1)S(1)}, bf16[16,1024]{1,0:T(8,128)(2,1)S(1)}, u32[]{:S(2)}, u32[]{:S(2)}) collective-permute-start(bf16[16,1024]{1,0:T(8,128)(2,1)S(1)} %slice.139), channel_id=1, source_target_pairs={{0,2},{1,3},{2,0},{3,1},{4,6},{5,7},{6,4},{7,5},{8,10},{9,11},{10,... | collective-permute-start | bytes 98312 | tf_op jit(solution)/shard_map/ppermute | solution.py:32
  211.6 21.6 %all-to-all-start.4 = ((bf16[8,2,16,1024]{3,2,1,0:T(8,128)(2,1)}), bf16[8,2,16,1024]{3,2,1,0:T(8,128)(2,1)S(1)}, u32[]{:S(2)}, u32[]{:S(2)}) async-start(bf16[8,2,16,1024]{3,2,1,0:T(8,128)(2,1)} %broadcast_in_dim.14), calls=%async_computation.4 | async-start | bytes 1048576 | tf_op jit(solution)/shard_map/all_to_all | solution.py:36
  234.1 34.4 %all-to-all-start.2 = ((bf16[8,2,32,512]{3,2,1,0:T(8,128)(2,1)}), bf16[8,2,32,512]{3,2,1,0:T(8,128)(2,1)S(1)}, u32[]{:S(2)}, u32[]{:S(2)}) async-start(bf16[8,2,32,512]{3,2,1,0:T(8,128)(2,1)} %broadcast_in_dim.12), calls=%async_computation.2 | async-start | bytes 1048576 | tf_op jit(solution)/shard_map/all_to_all | solution.py:36
  241.3 21.7 %collective-permute-start.30 = (bf16[8,2,16,1024]{3,2,1,0:T(8,128)(2,1)S(1)}, bf16[8,2,16,1024]{3,2,1,0:T(8,128)(2,1)S(1)}, u32[]{:S(2)}, u32[]{:S(2)}) collective-permute-start(bf16[8,2,16,1024]{3,2,1,0:T(8,128)(2,1)S(1)} %all-to-all-done.4.refs_0_), channel_id=1, source_target_pairs={{0,16},{1,17},{2,18},{3,19},{4,20},{5,21},{6,22},{7,23},{8,24},{9,... | collective-permute-start | bytes 1572872 | tf_op jit(solution)/shard_map/ppermute | solution.py:32
  264.6 52.8 %collective-permute-start.31 = (bf16[4,8,2,16,1024]{4,3,2,1,0:T(8,128)(2,1)}, bf16[4,8,2,16,1024]{4,3,2,1,0:T(8,128)(2,1)S(1)}, u32[]{:S(2)}, u32[]{:S(2)}) collective-permute-start(bf16[4,8,2,16,1024]{4,3,2,1,0:T(8,128)(2,1)} %pad_maximum_fusion.6), channel_id=1, source_target_pairs={{0,4},{1,5},{2,6},{3,7},{4,0},{5,1},{6,2},{7,3},{8,12},{9,13},{10,... | collective-permute-start | bytes 6291464 | tf_op jit(solution)/shard_map/ppermute | solution.py:32
  284.5 41.6 %collective-permute-start.22 = (bf16[3,8,2,32,512]{4,3,2,1,0:T(8,128)(2,1)}, bf16[3,8,2,32,512]{4,3,2,1,0:T(8,128)(2,1)}, u32[]{:S(2)}, u32[]{:S(2)}) collective-permute-start(bf16[3,8,2,32,512]{4,3,2,1,0:T(8,128)(2,1)} %pad_maximum_fusion.7), channel_id=1, source_target_pairs={{0,4},{1,5},{2,6},{3,7},{4,0},{5,1},{6,2},{7,3},{8,12},{9,13},{10,... | collective-permute-start | bytes 4718600 | tf_op jit(solution)/shard_map/ppermute | solution.py:32
  290.7 22.8 %collective-permute-start.11 = (bf16[256,1024]{1,0:T(8,128)(2,1)}, bf16[256,1024]{1,0:T(8,128)(2,1)}, u32[]{:S(2)}, u32[]{:S(2)}) collective-permute-start(bf16[256,1024]{1,0:T(8,128)(2,1)} %get-tuple-element.51), channel_id=1, source_target_pairs={{0,3},{1,2},{2,1},{3,0},{4,7},{5,6},{6,5},{7,4},{8,11},{9,10},{10,... | collective-permute-start | bytes 1572872 | tf_op jit(solution)/shard_map/ppermute | solution.py:32
  304.2 28.0 %collective-permute-start.19 = (bf16[8,2,32,512]{3,2,1,0:T(8,128)(2,1)S(1)}, bf16[8,2,32,512]{3,2,1,0:T(8,128)(2,1)S(1)}, u32[]{:S(2)}, u32[]{:S(2)}) collective-permute-start(bf16[8,2,32,512]{3,2,1,0:T(8,128)(2,1)S(1)} %collective-permute-done.18.refs_0_), channel_id=1, source_target_pairs={{0,4},{1,5},{2,6},{3,7},{4,0},{5,1},{6,2},{7,3},{8,12},{9,13},{10,... | collective-permute-start | bytes 1572872 | tf_op jit(solution)/shard_map/ppermute | solution.py:32
  (32 other events, 331.6 us)
